TPU v7x, 32 devices: a whole 2x2x4 slice. The times are simulated.
32 devices in a mesh: fs: 8 (over z, y), tp: 4 (over x, core).
Axes of the slice: x: 2, y: 2, z: 4, core: 2. Of those that a mesh axis runs over, the one named last changes fastest.
Arguments:
- tokens: bfloat16 [3072, 2048], P('fs'), may hold values from -6 to 6
- first_norm_scale: float32 [2048], replicated, may hold values from 0.1 to 1.9
- recurrent_branch_matrix: bfloat16 [2048, 1024], P('fs', 'tp'), may hold values from -0.125 to 0.125
- gelu_gate_matrix: bfloat16 [2048, 1024], P('fs', 'tp'), may hold values from -0.125 to 0.125
- filter_taps_weight: bfloat16 [4, 1024], P(None, 'tp'), may hold values from -3 to 3
- recurrence_gate_blocks: bfloat16 [16, 64, 64], P('tp'), may hold values from -0.75 to 0.75
- input_gate_blocks: bfloat16 [16, 64, 64], P('tp'), may hold values from -0.75 to 0.75
- base_decay_logits: float32 [1024], P('tp'), may hold values from 4 to 11
- extra_log_decay: float32 [3072, 1024], P('fs', 'tp'), may hold values from -0.7 to 0
- mixer_output_matrix: bfloat16 [2048, 1024], P('fs', 'tp'), may hold values from -0.5 to 0.5
- second_norm_scale: float32 [2048], replicated, may hold values from 0.1 to 1.9
- mixer_up_matrix: bfloat16 [2048, 4096], P('fs', 'tp'), may hold values from -0.125 to 0.125
- mixer_down_matrix: bfloat16 [2048, 4096], P('fs', 'tp'), may hold values from -0.09375 to 0.09375
Outputs:
- layer_out: bfloat16 [3072, 2048], P(('fs', 'tp'))
All inputs are finite; a program needn't handle non-finite values.
Results may differ from a plain program's by a relative error of at most 0.022.
Values may be sent and summed in bfloat16 or wider, within the bound.
A program may use at most 64 MiB of HBM per device.

v0:
```python
import jax
import jax.numpy as jnp
from jax import lax
from jax.sharding import PartitionSpec as P

epsilon = 1e-06
decay_rate_scale = 8.0


def rms_scaled(sequence_token_rows, scales):
    widened = sequence_token_rows.astype(jnp.float32)
    mean_square = jnp.mean(widened * widened, axis=-1, keepdims=True)
    return (widened * lax.rsqrt(mean_square + epsilon) * scales).astype(jnp.bfloat16)


def linear_combine(earlier, later):
    return (earlier[0] * later[0], later[0] * earlier[1] + later[1])


def causal_taps(branch, filter_taps_weight):
    tap_count = filter_taps_weight.shape[0]
    positions = branch.shape[0]
    padded = jnp.pad(branch.astype(jnp.float32), ((tap_count - 1, 0), (0, 0)))
    running = jnp.zeros(branch.shape, jnp.float32)
    for offset in range(tap_count):
        running = running + padded[offset : offset + positions] * filter_taps_weight[offset].astype(
            jnp.float32
        )
    return running.astype(jnp.bfloat16)


def block_map(convolved, blocks):
    positions, channels = convolved.shape
    grouped = convolved.reshape(positions, blocks.shape[0], blocks.shape[1])
    mapped = jnp.einsum("sgi,gij->sgj", grouped, blocks, preferred_element_type=jnp.float32)
    return jax.nn.sigmoid(mapped.reshape(positions, channels))


def contract_columns(left, right):
    return lax.dot_general(
        left, right, (((1,), (1,)), ((), ())), preferred_element_type=jnp.float32
    )


def local(
    tokens,
    first_norm_scale,
    recurrent_branch_matrix,
    gelu_gate_matrix,
    filter_taps_weight,
    recurrence_gate_blocks,
    input_gate_blocks,
    base_decay_logits,
    extra_log_decay,
    mixer_output_matrix,
    second_norm_scale,
    mixer_up_matrix,
    mixer_down_matrix,
):
    positions = tokens.shape[0]
    own_count = positions // lax.axis_size("tp")
    normed = rms_scaled(tokens, first_norm_scale)
    branch_sum = jnp.dot(
        normed,
        lax.all_gather(recurrent_branch_matrix, "fs", axis=0, tiled=True),
        preferred_element_type=jnp.float32,
    )
    gate_sum = jnp.dot(
        normed,
        lax.all_gather(gelu_gate_matrix, "fs", axis=0, tiled=True),
        preferred_element_type=jnp.float32,
    )
    branch = branch_sum.astype(jnp.bfloat16)
    gate_branch = gate_sum.astype(jnp.bfloat16)
    out_full = lax.all_gather(mixer_output_matrix, "fs", axis=0, tiled=True)
    convolved = causal_taps(branch, filter_taps_weight)
    recurrence_gate_value = block_map(convolved, recurrence_gate_blocks)
    admission = block_map(convolved, input_gate_blocks)
    log_keep_factor = (
        decay_rate_scale * recurrence_gate_value * jax.nn.log_sigmoid(base_decay_logits)
        + extra_log_decay
    )
    retain = jnp.exp(log_keep_factor)
    driven = jnp.sqrt(-jnp.expm1(2.0 * log_keep_factor)) * (
        admission * convolved.astype(jnp.float32)
    )
    memory = lax.associative_scan(linear_combine, (retain, driven), axis=0)[1]
    recurrent = (memory * jax.nn.gelu(gate_branch.astype(jnp.float32))).astype(jnp.bfloat16)
    up_full = lax.all_gather(mixer_up_matrix, "fs", axis=0, tiled=True)
    whole_sum = lax.psum(contract_columns(recurrent, out_full).astype(jnp.bfloat16), "tp").astype(
        jnp.float32
    )
    residual_all = (tokens.astype(jnp.float32) + whole_sum).astype(jnp.bfloat16)
    raised = jnp.dot(
        rms_scaled(residual_all, second_norm_scale), up_full, preferred_element_type=jnp.float32
    )
    hidden = jnp.square(jax.nn.relu(raised)).astype(jnp.bfloat16)
    residual = lax.dynamic_slice_in_dim(
        residual_all, lax.axis_index("tp") * own_count, own_count, 0
    )
    down_full = lax.all_gather(mixer_down_matrix, "fs", axis=0, tiled=True)
    channel_sum = lax.psum_scatter(
        contract_columns(hidden, down_full).astype(jnp.bfloat16),
        "tp",
        scatter_dimension=0,
        tiled=True,
    ).astype(jnp.float32)
    return (residual.astype(jnp.float32) + channel_sum).astype(jnp.bfloat16)


def solution(mesh):
    in_specs = (
        P("fs", None),
        P(),
        P("fs", "tp"),
        P("fs", "tp"),
        P(None, "tp"),
        P("tp", None, None),
        P("tp", None, None),
        P("tp"),
        P("fs", "tp"),
        P("fs", "tp"),
        P(),
        P("fs", "tp"),
        P("fs", "tp"),
    )
    out_specs = P(("fs", "tp"), None)
    return jax.shard_map(local, mesh=mesh, in_specs=in_specs, out_specs=out_specs, check_vma=False)
```

profile of v0, /device:TPU:0, one launch (start us, length us, event | category | flops | bytes accessed | tf_op | source)
XLA Modules:
  0.0 372.9 jit_solution(10167174261476025850)
XLA Ops:
  6.5 0.7 all-gather.6.cloned.1.call-update
  7.3 0.0 all-gather.10.cloned.1.call-start
  7.3 0.7 all-gather.10.cloned.1.call-update
  8.0 0.0 all-gather.8.cloned.1.call-start
  8.1 0.7 all-gather.8.cloned.1.call-update
  8.7 0.0 all-reduce.19.cloned.1.call-start
  8.8 0.8 slice_convert_fusion.3
  9.6 1.8 fusion.3
  11.4 0.7 fusion.59
  12.1 40.4 %all-gather.6.cloned.1.call-done = bf16[2048,256]{1,0:T(8,128)(2,1)} async-done(((bf16[256,256]{1,0:T(8,128)(2,1)}), bf16[2048,256]{1,0:T(8,128)(2,1)}) %all-gather.6.cloned.1.call-update) | async-done | bytes 1048592 | tf_op jit(solution)/shard_map/all_gather | solution.py:65
  52.5 2.3 fusion.20
  54.8 0.0 copy-start.2
  54.9 0.2 add_convert_fusion.1
  55.0 0.2 copy.20
  55.2 0.3 fusion.18
  55.5 0.2 copy.22
  55.7 0.3 fusion.15
  56.0 0.2 copy.24
  56.2 0.5 fusion.49
  56.7 0.1 slice.221
  56.8 0.1 slice.222
  57.0 0.1 slice.220
  57.1 0.1 slice.224
  57.2 0.1 fusion.66
  58.3 0.3 slice.278
  58.6 0.3 slice.219
  59.1 0.0 copy-start.1
  59.1 0.0 copy-start.4
  59.6 0.1 pad.69
  59.7 0.1 fusion.44
  59.7 0.1 pad.68
  59.8 33.8 %all-gather.10.cloned.1.call-done = bf16[2048,256]{1,0:T(8,128)(2,1)} async-done(((bf16[256,256]{1,0:T(8,128)(2,1)}), bf16[2048,256]{1,0:T(8,128)(2,1)}) %all-gather.10.cloned.1.call-update) | async-done | bytes 1048592 | tf_op jit(solution)/shard_map/all_gather | solution.py:75
  93.6 41.2 %all-gather.8.cloned.1.call-done = bf16[2048,256]{1,0:T(8,128)(2,1)} async-done(((bf16[256,256]{1,0:T(8,128)(2,1)}), bf16[2048,256]{1,0:T(8,128)(2,1)}) %all-gather.8.cloned.1.call-update) | async-done | bytes 1048592 | tf_op jit(solution)/shard_map/all_gather | solution.py:70
  134.8 4.6 %convolution_convert_fusion.1 = bf16[384,2048]{1,0:T(8,128)(2,1)} fusion(bf16[2048,256]{1,0:T(8,128)(2,1)} %all-gather.10.cloned.1.call-done, bf16[2048,256]{1,0:T(8,128)(2,1)} %all-gather.8.cloned.1.call-done, bf16[384,2048]{1,0:T(8,128)(2,1)S(1)} %copy-done.1, f32[2048]{0:T(1024)S(1)} %copy-done.4, f32[384]{0:T(512)S(1)} %add_rsqrt_fusion.1, ...), kind=kOutput, calls=%fused_computation.13 | convolution fusion | flops 810516480 | bytes 6039040 | tf_op jit(solution)/shard_map/dot_general | solution.py:40
  139.4 0.0 all-reduce.19.cloned.1.call-update
  139.5 0.0 all-gather.12.cloned.1.call-start
  139.5 0.5 all-gather.12.cloned.1.call-update
  140.1 0.0 all-gather.14.cloned.1.call-start
  140.1 0.5 all-gather.14.cloned.1.call-update
  140.6 0.0 reduce-scatter.2.cloned.1.call-start
  140.7 40.5 %all-reduce.19.cloned.1.call-done = bf16[384,2048]{1,0:T(8,128)(2,1)} async-done(((bf16[384,2048]{1,0:T(8,128)(2,1)}), bf16[384,2048]{1,0:T(8,128)(2,1)}) %all-reduce.19.cloned.1.call-update) | async-done | bytes 1572880 | tf_op jit(solution)/shard_map/psum | solution.py:90
  181.2 2.1 fusion
  183.3 72.7 %all-gather.12.cloned.1.call-done = bf16[2048,1024]{1,0:T(8,128)(2,1)} async-done(((bf16[256,1024]{1,0:T(8,128)(2,1)}), bf16[2048,1024]{1,0:T(8,128)(2,1)}) %all-gather.12.cloned.1.call-update) | async-done | bytes 4194320 | tf_op jit(solution)/shard_map/all_gather | solution.py:89
  256.0 73.3 %all-gather.14.cloned.1.call-done = bf16[2048,1024]{1,0:T(8,128)(2,1)} async-done(((bf16[256,1024]{1,0:T(8,128)(2,1)}), bf16[2048,1024]{1,0:T(8,128)(2,1)}) %all-gather.14.cloned.1.call-update) | async-done | bytes 4194320 | tf_op jit(solution)/shard_map/all_gather | solution.py:101
  329.4 8.1 %convolution_convert_fusion = bf16[384,2048]{1,0:T(8,128)(2,1)} fusion(bf16[2048,1024]{1,0:T(8,128)(2,1)} %all-gather.14.cloned.1.call-done, bf16[2048,1024]{1,0:T(8,128)(2,1)} %all-gather.12.cloned.1.call-done, bf16[384,2048]{1,0:T(8,128)(2,1)S(1)} %get-tuple-element.6, f32[2048]{0:T(1024)S(1)} %copy-done.5, f32[384]{0:T(512)S(1)} %add_rsqrt_fusion), kind=kOutput, calls=%fused_computation.12 | convolution fusion | flops 3226337280 | bytes 11544064 | tf_op jit(solution)/shard_map/dot_general | solution.py:40
  337.5 0.0 reduce-scatter.2.cloned.1.call-update
  337.6 26.7 %reduce-scatter.2.cloned.1.call-done = bf16[96,2048]{1,0:T(8,128)(2,1)} async-done(((bf16[384,2048]{1,0:T(8,128)(2,1)}), bf16[96,2048]{1,0:T(8,128)(2,1)}) %reduce-scatter.2.cloned.1.call-update) | async-done | bytes 393232 | tf_op jit(solution)/shard_map/reduce_scatter | solution.py:102
  364.2 1.8 add_convert_fusion
  (96 shorter events, 1.3 us)
Async XLA Ops:
  6.5 48.7 %copy-start = (bf16[4,64,64]{2,1,0:T(8,128)(2,1)S(1)}, bf16[4,64,64]{2,1,0:T(8,128)(2,1)}, u32[]{:S(2)}) copy-start(bf16[4,64,64]{2,1,0:T(8,128)(2,1)} %param.18) | copy-start | bytes 98308
  6.5 46.0 %all-gather.6.cloned.1.call-start = ((), (), s32[]{:S(2)}) async-start(), calls=%async_computation.1 | async-start | bytes 1179648 | tf_op jit(solution)/shard_map/all_gather | solution.py:65
  7.3 86.4 %all-gather.10.cloned.1.call-start = ((), (), s32[]{:S(2)}) async-start(), calls=%async_computation.3 | async-start | bytes 1179648 | tf_op jit(solution)/shard_map/all_gather | solution.py:75
  8.0 126.8 %all-gather.8.cloned.1.call-start = ((), (), s32[]{:S(2)}) async-start(), calls=%async_computation.2 | async-start | bytes 1179648 | tf_op jit(solution)/shard_map/all_gather | solution.py:70
  8.7 172.4 %all-reduce.19.cloned.1.call-start = ((), (), s32[]{:S(2)}) async-start(), calls=%async_computation.4 | async-start | bytes 3145728 | tf_op jit(solution)/shard_map/psum | solution.py:90
  12.1 43.6 %copy-start.3 = (bf16[4,64,64]{2,1,0:T(8,128)(2,1)S(1)}, bf16[4,64,64]{2,1,0:T(8,128)(2,1)}, u32[]{:S(2)}) copy-start(bf16[4,64,64]{2,1,0:T(8,128)(2,1)} %param.19) | copy-start | bytes 98308
  54.8 1.4 copy-start.2
  59.1 75.7 %copy-start.1 = (bf16[384,2048]{1,0:T(8,128)(2,1)S(1)}, bf16[384,2048]{1,0:T(8,128)(2,1)}, u32[]{:S(2)}) copy-start(bf16[384,2048]{1,0:T(8,128)(2,1)} %param.13) | copy-start | bytes 4718596
  59.1 75.7 %copy-start.4 = (f32[2048]{0:T(1024)S(1)}, f32[2048]{0:T(1024)}, u32[]{:S(2)}) copy-start(f32[2048]{0:T(1024)} %param.14) | copy-start | bytes 24580
  139.5 189.9 %copy-start.5 = (f32[2048]{0:T(1024)S(1)}, f32[2048]{0:T(1024)}, u32[]{:S(2)}) copy-start(f32[2048]{0:T(1024)} %param.23) | copy-start | bytes 24580
  139.5 116.6 %all-gather.12.cloned.1.call-start = ((), (), s32[]{:S(2)}) async-start(), calls=%async_computation.5 | async-start | bytes 4718592 | tf_op jit(solution)/shard_map/all_gather | solution.py:89
  140.1 189.3 %all-gather.14.cloned.1.call-start = ((), (), s32[]{:S(2)}) async-start(), calls=%async_computation.6 | async-start | bytes 4718592 | tf_op jit(solution)/shard_map/all_gather | solution.py:101
  140.6 223.6 %reduce-scatter.2.cloned.1.call-start = ((), (), s32[]{:S(2)}) async-start(), calls=%async_computation.7 | async-start | bytes 1966080 | tf_op jit(solution)/shard_map/reduce_scatter | solution.py:102
Sparse Core Ops, SparseCore 0:
  9.5 42.9 all-gather.5
  54.6 38.9 all-gather.9
  95.8 38.9 all-gather.7
  139.6 41.5 all-reduce.18
  183.2 72.8 all-gather.11
  258.0 71.3 all-gather.13
  337.7 26.5 reduce-scatter.1
where the time goes:
time: 373 us
  waiting for transfers between devices  332 us (89%)
  matrix products  15.7 us (4%)
  between operations  14.1 us (4%)
  other arithmetic  8.42 us (2%)
    all_gather x1, waiting for transfers between devices, local(): down_full = lax.all_gather(mixer_down_matrix, 'fs', axis=0, tiled=True)  73.3 us
    all_gather x1, waiting for transfers between devices, local(): up_full = lax.all_gather(mixer_up_matrix, 'fs', axis=0, tiled=True)  72.7 us
    all_gather x1, waiting for transfers between devices, local(): lax.all_gather(gelu_gate_matrix, 'fs', axis=0, tiled=True)  41.2 us
    psum x1, waiting for transfers between devices, local(): lax.psum(contract_columns(recurrent, out_full).astype(jnp.bfloat16), 'tp')  40.5 us
    all_gather x1, waiting for transfers between devices, local(): lax.all_gather(recurrent_branch_matrix, 'fs', axis=0, tiled=True)  40.4 us
    all_gather x1, waiting for transfers between devices, local(): out_full = lax.all_gather(mixer_output_matrix, 'fs', axis=0, tiled=True)  33.8 us
    reduce_scatter x1, waiting for transfers between devices, local(): lax.psum_scatter(contract_columns(hidden, down_full).astype(jnp.bfloat16)...  26.7 us
    dot_general x2, matrix products, contract_columns(): lax.dot_general(left, right, (((1,), (1,)), ((), ())), preferred_element_...  12.8 us
  transfers between devices with their start and end apart: 7, of which 7 were waited for; matrix products, arithmetic and copies ran while one was open for 3% of the time, Pallas kernels for 0%

commit v1 on v0

--- a/solution.py
+++ b/solution.py
@@ -72,7 +72,6 @@
     )
     branch = branch_sum.astype(jnp.bfloat16)
     gate_branch = gate_sum.astype(jnp.bfloat16)
-    out_full = lax.all_gather(mixer_output_matrix, "fs", axis=0, tiled=True)
     convolved = causal_taps(branch, filter_taps_weight)
     recurrence_gate_value = block_map(convolved, recurrence_gate_blocks)
     admission = block_map(convolved, input_gate_blocks)
@@ -86,7 +85,16 @@
     )
     memory = lax.associative_scan(linear_combine, (retain, driven), axis=0)[1]
     recurrent = (memory * jax.nn.gelu(gate_branch.astype(jnp.float32))).astype(jnp.bfloat16)
-    up_full = lax.all_gather(mixer_up_matrix, "fs", axis=0, tiled=True)
+
+    def _prepare_sheet(frame_in, array_in):
+        b_next = jnp.split(
+            jax.lax.all_gather(jnp.concatenate([frame_in, array_in], 1), "fs", axis=0, tiled=True),
+            [frame_in.shape[1]],
+            1,
+        )
+        return b_next
+
+    out_full, up_full = _prepare_sheet(mixer_output_matrix, mixer_up_matrix)
     whole_sum = lax.psum(contract_columns(recurrent, out_full).astype(jnp.bfloat16), "tp").astype(
         jnp.float32
     )

time: 373 us -> 345 us (0.925)
  waiting for transfers between devices: 332 us -> 302 us
    all_gather x2 -> x1, waiting for transfers between devices: 107 us -> 86.8 us  [_prepare_sheet(): jax.lax.all_gather(jnp.concatenate([frame_in, array_in], 1), 'fs', axis=0...]
    all_gather x1, waiting for transfers between devices: 41.2 us -> 31 us  [local(): lax.all_gather(gelu_gate_matrix, 'fs', axis=0, tiled=True)]
  transfers between devices with their start and end apart: 7 -> 6, of which waited for: 7 -> 6; matrix products, arithmetic and copies ran while one was open for 3% -> 4% of each run, Pallas kernels for 0% -> 0%
where the time goes in v1:
time: 345 us
  waiting for transfers between devices  302 us (88%)
  matrix products  15.1 us (4%)
  between operations  14.1 us (4%)
  other arithmetic  9.5 us (3%)
  local copies, waits for them, and re-layouts  4.06 us (1%)
    all_gather x1, waiting for transfers between devices, _prepare_sheet(): jax.lax.all_gather(jnp.concatenate([frame_in, array_in], 1), 'fs', axis=0...  86.8 us
    all_gather x1, waiting for transfers between devices, local(): down_full = lax.all_gather(mixer_down_matrix, 'fs', axis=0, tiled=True)  72.7 us
    all_gather x1, waiting for transfers between devices, local(): lax.all_gather(recurrent_branch_matrix, 'fs', axis=0, tiled=True)  41.9 us
    psum x1, waiting for transfers between devices, local(): lax.psum(contract_columns(recurrent, out_full).astype(jnp.bfloat16), 'tp')  40.6 us
    all_gather x1, waiting for transfers between devices, local(): lax.all_gather(gelu_gate_matrix, 'fs', axis=0, tiled=True)  31 us
    reduce_scatter x1, waiting for transfers between devices, local(): lax.psum_scatter(contract_columns(hidden, down_full).astype(jnp.bfloat16)...  26.7 us
    dot_general x2, matrix products, contract_columns(): lax.dot_general(left, right, (((1,), (1,)), ((), ())), preferred_element_...  12.6 us
  transfers between devices with their start and end apart: 6, of which 6 were waited for; matrix products, arithmetic and copies ran while one was open for 4% of the time, Pallas kernels for 0%

profile of v1, /device:TPU:0, one launch (start us, length us, event | category | flops | bytes accessed | tf_op | source)
XLA Modules:
  0.0 344.6 jit_solution(11411139586150388234)
XLA Ops:
  6.5 0.0 copy-start
  6.5 0.0 all-gather.5.cloned.1.call-start
  6.6 0.7 all-gather.5.cloned.1.call-update
  7.3 0.0 all-gather.7.cloned.1.call-start
  7.3 0.7 all-gather.7.cloned.1.call-update
  8.0 0.0 all-gather.9.cloned.1.call-start
  8.1 2.0 pad_maximum_fusion
  10.0 0.0 all-gather.9.cloned.1.call-update
  10.1 0.0 all-reduce.19.cloned.1.call-start
  10.1 0.0 copy-done.1
  10.1 0.4 fusion.5
  10.5 0.0 copy-done.3
  10.6 0.0 copy-done.2
  10.6 0.0 copy-start.4
  10.6 41.9 %all-gather.5.cloned.1.call-done = bf16[2048,256]{1,0:T(8,128)(2,1)} async-done(((bf16[256,256]{1,0:T(8,128)(2,1)}), bf16[2048,256]{1,0:T(8,128)(2,1)}) %all-gather.5.cloned.1.call-update) | async-done | bytes 1048592 | tf_op jit(solution)/shard_map/all_gather | solution.py:65
  52.5 1.8 fusion.23
  54.4 0.2 add_convert_fusion.1
  54.6 0.2 copy.20
  54.7 0.3 fusion.21
  55.0 0.2 copy.22
  55.2 0.3 fusion.18
  55.5 0.9 copy.24
  56.5 1.6 fusion.56
  58.0 0.1 slice.221
  58.2 0.1 slice.222
  58.3 0.1 slice.220
  58.5 0.7 slice.224
  59.2 1.0 fusion.73
  61.2 0.3 slice.278
  61.5 0.3 slice.219
  62.5 0.1 pad.69
  62.5 0.1 fusion.51
  62.6 0.1 pad.68
  62.7 31.0 %all-gather.7.cloned.1.call-done = bf16[2048,256]{1,0:T(8,128)(2,1)} async-done(((bf16[256,256]{1,0:T(8,128)(2,1)}), bf16[2048,256]{1,0:T(8,128)(2,1)}) %all-gather.7.cloned.1.call-update) | async-done | bytes 1048592 | tf_op jit(solution)/shard_map/all_gather | solution.py:70
  93.7 86.8 %all-gather.9.cloned.1.call-done = bf16[2048,1280]{1,0:T(8,128)(2,1)} async-done(((bf16[256,1280]{1,0:T(8,128)(2,1)}), bf16[2048,1280]{1,0:T(8,128)(2,1)}) %all-gather.9.cloned.1.call-update) | async-done | bytes 5242896 | tf_op jit(solution)/shard_map/all_gather | solution.py:91
  180.5 4.6 %convolution_convert_fusion.1 = bf16[384,2048]{1,0:T(8,128)(2,1)} fusion(bf16[2048,1280]{1,0:T(8,128)(2,1)} %all-gather.9.cloned.1.call-done, bf16[2048,256]{1,0:T(8,128)(2,1)} %all-gather.7.cloned.1.call-done, bf16[384,2048]{1,0:T(8,128)(2,1)S(1)} %copy-done.1, f32[2048]{0:T(1024)S(1)} %copy-done.5, f32[384]{0:T(512)S(1)} %add_rsqrt_fusion.1, ...), kind=kOutput, calls=%fused_computation.15 | convolution fusion | flops 810516480 | bytes 6039040 | tf_op jit(solution)/shard_map/dot_general | solution.py:40
  185.1 0.0 all-reduce.19.cloned.1.call-update
  185.1 0.0 all-gather.11.cloned.1.call-start
  185.1 0.5 all-gather.11.cloned.1.call-update
  185.7 0.0 reduce-scatter.2.cloned.1.call-start
  185.7 40.6 %all-reduce.19.cloned.1.call-done = bf16[384,2048]{1,0:T(8,128)(2,1)} async-done(((bf16[384,2048]{1,0:T(8,128)(2,1)}), bf16[384,2048]{1,0:T(8,128)(2,1)}) %all-reduce.19.cloned.1.call-update) | async-done | bytes 1572880 | tf_op jit(solution)/shard_map/psum | solution.py:98
  226.3 2.1 fusion.2
  228.4 72.7 %all-gather.11.cloned.1.call-done = bf16[2048,1024]{1,0:T(8,128)(2,1)} async-done(((bf16[256,1024]{1,0:T(8,128)(2,1)}), bf16[2048,1024]{1,0:T(8,128)(2,1)}) %all-gather.11.cloned.1.call-update) | async-done | bytes 4194320 | tf_op jit(solution)/shard_map/all_gather | solution.py:109
  301.1 0.0 copy-done.6
  301.1 8.1 %convolution_convert_fusion = bf16[384,2048]{1,0:T(8,128)(2,1)} fusion(bf16[2048,1024]{1,0:T(8,128)(2,1)} %all-gather.11.cloned.1.call-done, bf16[2048,1280]{1,0:T(8,128)(2,1)} %all-gather.9.cloned.1.call-done, bf16[384,2048]{1,0:T(8,128)(2,1)S(1)} %get-tuple-element.6, f32[2048]{0:T(1024)S(1)} %copy-done.6, f32[384]{0:T(512)S(1)} %add_rsqrt_fusion), kind=kOutput, calls=%fused_computation.14 | convolution fusion | flops 3226337280 | bytes 11544064 | tf_op jit(solution)/shard_map/dot_general | solution.py:40
  309.2 0.0 reduce-scatter.2.cloned.1.call-update
  309.2 26.7 %reduce-scatter.2.cloned.1.call-done = bf16[96,2048]{1,0:T(8,128)(2,1)} async-done(((bf16[384,2048]{1,0:T(8,128)(2,1)}), bf16[96,2048]{1,0:T(8,128)(2,1)}) %reduce-scatter.2.cloned.1.call-update) | async-done | bytes 393232 | tf_op jit(solution)/shard_map/reduce_scatter | solution.py:110
  335.9 1.8 add_convert_fusion
  (96 shorter events, 1.3 us)
Async XLA Ops:
  6.5 48.2 %copy-start = (bf16[4,64,64]{2,1,0:T(8,128)(2,1)S(1)}, bf16[4,64,64]{2,1,0:T(8,128)(2,1)}, u32[]{:S(2)}) copy-start(bf16[4,64,64]{2,1,0:T(8,128)(2,1)} %param.18) | copy-start | bytes 98308
  6.5 3.6 %copy-start.1 = (bf16[384,2048]{1,0:T(8,128)(2,1)S(1)}, bf16[384,2048]{1,0:T(8,128)(2,1)}, u32[]{:S(2)}) copy-start(bf16[384,2048]{1,0:T(8,128)(2,1)} %param.13) | copy-start | bytes 4718596
  6.5 4.0 %copy-start.3 = (f32[256]{0:T(256)S(1)}, f32[256]{0:T(256)}, u32[]{:S(2)}) copy-start(f32[256]{0:T(256)} %param.20) | copy-start | bytes 3076
  6.5 4.0 %copy-start.2 = (bf16[4,256]{1,0:T(4,128)(2,1)S(1)}, bf16[4,256]{1,0:T(4,128)(2,1)}, u32[]{:S(2)}) copy-start(bf16[4,256]{1,0:T(4,128)(2,1)} %param.17) | copy-start | bytes 6148
  6.5 46.0 %copy-start.5 = (f32[2048]{0:T(1024)S(1)}, f32[2048]{0:T(1024)}, u32[]{:S(2)}) copy-start(f32[2048]{0:T(1024)} %param.14) | copy-start | bytes 24580
  6.5 46.0 %all-gather.5.cloned.1.call-start = ((), (), s32[]{:S(2)}) async-start(), calls=%async_computation.1 | async-start | bytes 1179648 | tf_op jit(solution)/shard_map/all_gather | solution.py:65
  7.3 86.4 %all-gather.7.cloned.1.call-start = ((), (), s32[]{:S(2)}) async-start(), calls=%async_computation.2 | async-start | bytes 1179648 | tf_op jit(solution)/shard_map/all_gather | solution.py:70
  8.0 172.4 %all-gather.9.cloned.1.call-start = ((), (), s32[]{:S(2)}) async-start(), calls=%async_computation.3 | async-start | bytes 5898240 | tf_op jit(solution)/shard_map/all_gather | solution.py:91
  10.1 216.2 %all-reduce.19.cloned.1.call-start = ((), (), s32[]{:S(2)}) async-start(), calls=%async_computation.4 | async-start | bytes 3145728 | tf_op jit(solution)/shard_map/psum | solution.py:98
  10.6 44.6 %copy-start.4 = (bf16[4,64,64]{2,1,0:T(8,128)(2,1)S(1)}, bf16[4,64,64]{2,1,0:T(8,128)(2,1)}, u32[]{:S(2)}) copy-start(bf16[4,64,64]{2,1,0:T(8,128)(2,1)} %param.19) | copy-start | bytes 98308
  185.1 116.1 %copy-start.6 = (f32[2048]{0:T(1024)S(1)}, f32[2048]{0:T(1024)}, u32[]{:S(2)}) copy-start(f32[2048]{0:T(1024)} %param.23) | copy-start | bytes 24580
  185.1 116.1 %all-gather.11.cloned.1.call-start = ((), (), s32[]{:S(2)}) async-start(), calls=%async_computation.5 | async-start | bytes 4718592 | tf_op jit(solution)/shard_map/all_gather | solution.py:109
  185.7 150.3 %reduce-scatter.2.cloned.1.call-start = ((), (), s32[]{:S(2)}) async-start(), calls=%async_computation.6 | async-start | bytes 1966080 | tf_op jit(solution)/shard_map/reduce_scatter | solution.py:110
Sparse Core Ops, SparseCore 0:
  9.5 42.9 all-gather.4
  54.6 38.9 all-gather.6
  95.9 84.5 all-gather.8
  185.2 41.0 all-reduce.18
  228.3 72.8 all-gather.10
  309.4 26.5 reduce-scatter.1
